TPU v7x, 32 devices: a whole 2x2x4 slice. The times are simulated.
32 devices in a mesh: ep: 8 (over z, x), tp: 4 (over y, core).
Axes of the slice: x: 2, y: 2, z: 4, core: 2. Of those that a mesh axis runs over, the one named last changes fastest.
Arguments:
- hidden: bfloat16 [32, 2048], P('ep'), may hold values from -6 to 6
- attn_gain: float32 [2048], replicated, may hold values from 0.3 to 3
- query_weight: bfloat16 [2048, 2048], P('ep', 'tp'), may hold values from -0.125 to 0.125
- head_bias: float32 [16], replicated, may hold values from -10 to -4
- key_cache: bfloat16 [32, 4, 1024, 128], P('ep', 'tp'), may hold values from -6 to 6
- value_cache: bfloat16 [32, 4, 1024, 128], P('ep', 'tp'), may hold values from -7 to 7
- lengths: int32 [32], P('ep'), may hold values from 256 to 1024, as said below
- out_weight: bfloat16 [2048, 2048], P('tp', 'ep'), may hold values from -0.125 to 0.125
- moe_gain: float32 [2048], replicated, may hold values from 0.1 to 1.9
- route_group: int32 [32], P('ep'), may hold values from 0 to 1, as said below
- route_inner: int32 [32, 2], P('ep'), may hold values from 0 to 3, as said below
- route_weight: bfloat16 [32, 2], P('ep'), may hold values from 0.25 to 1
- gate_w: bfloat16 [8, 2048, 768], P('ep', None, 'tp'), may hold values from -0.125 to 0.125
- up_w: bfloat16 [8, 2048, 768], P('ep', None, 'tp'), may hold values from -0.125 to 0.125
- down_w: bfloat16 [8, 768, 2048], P('ep', 'tp'), may hold values from -0.21875 to 0.21875
Outputs:
- mixed: bfloat16 [32, 2048], P('ep', 'tp')
Inputs may be any that keep to these rules, and one draw needn't show every extreme that they name: `lengths`: some sequence has length 1024 in every draw. Within the rows of one device (aligned blocks of 4 rows) no expert route_group * 4 + route_inner is named twice; one expert is named in every block. `route_inner`: the 2 entries of a row differ.
All inputs are finite; a program needn't handle non-finite values.
Results may differ from a plain program's by a relative error of at most 0.013.
Values may be sent and summed in bfloat16 or wider, within the bound.
A program may use at most 64 MiB of HBM per device.

v0:
```python
import jax
import jax.numpy as jnp
from jax import lax
from jax.sharding import PartitionSpec as P

rms_epsilon = 1e-06


def rms_scale(values, gain):
    wide = values.astype(jnp.float32)
    scaled = wide * lax.rsqrt(jnp.mean(wide * wide, axis=-1, keepdims=True) + rms_epsilon)
    return (scaled * gain).astype(jnp.bfloat16)


def body(
    hidden,
    attn_gain,
    query_weight,
    head_bias,
    key_cache,
    value_cache,
    lengths,
    out_weight,
    moe_gain,
    route_group,
    route_inner,
    route_weight,
    gate_w,
    up_w,
    down_w,
):
    n_tp = lax.axis_size("tp")
    n_ep = lax.axis_size("ep")
    tokens = hidden.shape[0]
    d_model = hidden.shape[1]
    normed = rms_scale(hidden, attn_gain)
    feature_block = lax.all_to_all(normed, "ep", split_axis=1, concat_axis=0, tiled=True)
    queries = lax.psum_scatter(
        jnp.dot(feature_block, query_weight, preferred_element_type=jnp.float32),
        "ep",
        scatter_dimension=0,
        tiled=True,
    ).astype(jnp.bfloat16)
    head_size = key_cache.shape[3]
    local_kv = key_cache.shape[1]
    cache_len = key_cache.shape[2]
    local_heads = queries.shape[1] // head_size
    group_heads = local_heads // local_kv
    queries = queries.reshape(tokens, local_kv, group_heads, head_size)
    own_bias = lax.dynamic_slice_in_dim(
        head_bias, lax.axis_index("tp") * local_heads, local_heads, 0
    )
    own_bias = own_bias.reshape(local_kv, group_heads)
    scores = jnp.einsum(
        "tkgd,tkpd->tkgp", queries, key_cache, preferred_element_type=jnp.float32
    ) * head_size ** (-0.5)
    scores = scores + own_bias[None, :, :, None]
    position = jnp.arange(cache_len, dtype=jnp.int32)
    visible = position[None, None, None, :] < lengths[:, None, None, None]
    log_keep = jnp.where(visible, jax.nn.log_sigmoid(-scores), 0.0)
    later_sum = lax.cumsum(log_keep, axis=3, reverse=True) - log_keep
    weight = jnp.where(visible, jnp.exp(jax.nn.log_sigmoid(scores) + later_sum), 0.0).astype(
        jnp.bfloat16
    )
    heads_out = jnp.einsum(
        "tkgp,tkpd->tkgd", weight, value_cache, preferred_element_type=jnp.float32
    )
    heads_out = heads_out.astype(jnp.bfloat16).reshape(tokens, -1)
    partial_value = jnp.dot(
        heads_out,
        lax.all_gather(out_weight, "ep", axis=1, tiled=True),
        preferred_element_type=jnp.float32,
    )
    rounded = lax.optimization_barrier(partial_value.astype(jnp.bfloat16)).astype(jnp.float32)
    attended = lax.psum(rounded.astype(jnp.bfloat16), "tp").astype(jnp.float32)
    residual = (hidden.astype(jnp.float32) + attended).astype(jnp.bfloat16)
    normed_two = rms_scale(residual, moe_gain)
    per_device = gate_w.shape[0]
    experts = per_device * n_ep
    group_count = max(2, experts // 32)
    group_size = experts // group_count
    chosen = route_group[:, None] * group_size + route_inner
    matches = chosen[:, :, None] == jnp.arange(experts, dtype=jnp.int32)[None, None, :]
    picked = jnp.any(matches, axis=1).astype(jnp.bfloat16)
    mixing = jnp.sum(
        jnp.where(matches, route_weight[:, :, None].astype(jnp.float32), 0.0), axis=1
    ).astype(jnp.bfloat16)
    part_width = d_model // n_tp
    outgoing = jnp.einsum("te,td->ed", picked, normed_two, preferred_element_type=jnp.float32)
    outgoing = outgoing.astype(jnp.bfloat16).reshape(n_ep, per_device, d_model)
    arrived = lax.all_to_all(outgoing, "ep", split_axis=0, concat_axis=0, tiled=True)
    gated_in = jnp.einsum("sed,edf->sef", arrived, gate_w, preferred_element_type=jnp.float32)
    up_proj = jnp.einsum("sed,edf->sef", arrived, up_w, preferred_element_type=jnp.float32)
    activated = (jax.nn.silu(gated_in) * up_proj).astype(jnp.bfloat16)
    down_out = jnp.einsum("sef,efd->sed", activated, down_w, preferred_element_type=jnp.float32)
    down_rounded = lax.optimization_barrier(down_out.astype(jnp.bfloat16)).astype(jnp.float32)
    summed = lax.psum_scatter(
        down_rounded.astype(jnp.bfloat16), "tp", scatter_dimension=2, tiled=True
    )
    returned = lax.all_to_all(summed, "ep", split_axis=0, concat_axis=0, tiled=True).reshape(
        experts, part_width
    )
    routed = jnp.dot(mixing, returned, preferred_element_type=jnp.float32)
    own_residual = lax.dynamic_slice_in_dim(
        residual, lax.axis_index("tp") * part_width, part_width, 1
    )
    return (own_residual.astype(jnp.float32) + routed).astype(jnp.bfloat16)


def solution(mesh):
    placed = (
        P("ep", None),
        P(),
        P("ep", "tp"),
        P(),
        P("ep", "tp", None, None),
        P("ep", "tp", None, None),
        P("ep"),
        P("tp", "ep"),
        P(),
        P("ep"),
        P("ep", None),
        P("ep", None),
        P("ep", None, "tp"),
        P("ep", None, "tp"),
        P("ep", "tp", None),
    )
    return jax.shard_map(body, mesh=mesh, in_specs=placed, out_specs=P("ep", "tp"), check_vma=False)
```

profile of v0, /device:TPU:0, one launch (start us, length us, event | category | flops | bytes accessed | tf_op | source)
XLA Modules:
  0.0 150.5 jit_solution(8893848438040312585)
XLA Ops:
  6.5 0.0 copy-start
  6.5 0.0 all-gather.2.cloned.1.call-start
  6.5 0.7 all-gather.2.cloned.1.call-update
  7.3 0.8 fusion.25
  8.1 1.4 fusion.27
  9.5 7.3 %all-to-all-start = ((bf16[4,8,256]{2,0,1:T(4,128)(2,1)}), bf16[4,8,256]{2,0,1:T(4,128)(2,1)S(1)}, u32[]{:S(2)}, u32[]{:S(2)}) async-start(bf16[4,8,256]{2,0,1:T(4,128)(2,1)} %bitcast), calls=%async_computation | async-start | bytes 32768 | tf_op jit(solution)/shard_map/all_to_all | solution.py:37
  16.8 0.0 reduce-scatter.2.cloned.1.call-start
  16.8 0.7 broadcast_multiply_fusion
  17.5 0.7 broadcast_add_fusion
  18.2 0.0 copy-start.6
  18.2 0.7 iota_compare_fusion
  18.9 0.0 copy-start.5
  18.9 0.6 fusion.51
  19.5 0.7 dynamic_slice.6
  20.2 1.3 dynamic-slice
  22.1 1.4 all-to-all-done
  23.5 0.0 copy-done.6
  23.5 1.1 fusion.57
  24.6 37.7 %all-reduce = bf16[32,512]{1,0:T(8,128)(2,1)S(1)} all-reduce(f32[32,512]{1,0:T(8,128)S(1)} %fusion.57), channel_id=2, replica_groups=mesh['ep'=8,'tp'=4] {'ep'}, use_global_device_ids=true, to_apply=%region_1.0.clone | all-reduce | flops 16384 | bytes 98304
  62.3 0.0 copy-done
  62.3 0.4 fusion.21
  62.7 0.0 copy-done.5
  62.8 0.0 copy-start.4
  62.8 19.8 %reduce-window.6 = f32[4,1,4,8,128]{4,3,2,1,0:T(8,128)S(1)} reduce-window(f32[4,1,4,8,128]{4,3,2,1,0:T(8,128)S(1)} %bitcast.82, f32[]{:T(128)} %constant.12.clone.1), window={size=1x1x1x1x128 pad=0_0x0_0x0_0x0_0x0_127}, to_apply=%region_2.3 | reduce-window | flops 2080768 | bytes 131076 | tf_op jit(solution)/shard_map/reduce-window
  82.6 0.1 slice_reduce_fusion
  82.7 0.7 reduce-window.9
  83.4 0.1 slice_bitcast_fusion
  83.5 0.0 copy-start.1
  83.5 0.1 broadcast.72
  83.6 0.7 reshape.151
  84.3 0.0 copy-start.2
  84.3 0.0 copy-start.3
  84.3 2.4 %fusion.6 = bf16[1,4,4,128]{3,2,1,0:T(4,128)(2,1)} fusion(bf16[4,1,1024,128]{3,2,1,0:T(8,128)(2,1)} %param.20, f32[4,4,1024]{2,1,0:T(4,128)S(1)} %reshape.148, f32[4,4,1024]{2,1,0:T(4,128)} %reshape.151, f32[4,4,1024]{2,1,0:T(4,128)S(1)} %get-tuple-element.8, pred[4,1024]{1,0:T(4,128)(4,1)} %copy-done.5), kind=kOutput, calls=%fused_computation.14 | convolution fusion | flops 4540416 | bytes 1253376 | tf_op jit(solution)/shard_map/tkgp,tkpd->tkgd/dot_general | solution.py:65
  86.6 0.0 copy-start.8
  86.6 0.0 copy-start.7
  86.6 0.0 all-gather.2.cloned.1.call-done
  86.6 2.0 %convolution_convert_fusion.2 = bf16[4,2048]{1,0:T(4,128)(2,1)S(1)} fusion(bf16[512,2048]{1,0:T(8,128)(2,1)} %all-gather.2.cloned.1.call-done, bf16[1,4,4,128]{3,2,1,0:T(4,128)(2,1)} %fusion.6), kind=kOutput, calls=%fused_computation.4 | convolution fusion | flops 8396800 | bytes 2117632 | tf_op jit(solution)/shard_map/dot_general | solution.py:69
  88.6 10.1 %psum.7 = bf16[4,2048]{1,0:T(4,128)(2,1)S(1)} all-reduce(bf16[4,2048]{1,0:T(4,128)(2,1)S(1)} %convolution_convert_fusion.2), channel_id=1, replica_groups=mesh['ep'=8,'tp'=4] {'tp'}, use_global_device_ids=true, to_apply=%region_4.5 | all-reduce | flops 8192 | bytes 32768 | tf_op jit(solution)/shard_map/psum | solution.py:75
  98.7 0.0 copy-done.4
  98.7 0.1 fusion.22
  98.9 0.9 fusion
  99.8 0.5 broadcast.80
  100.3 0.7 reduce.2
  101.0 9.1 %all_to_all.29 = bf16[8,2,1024]{2,1,0:T(2,128)(2,1)S(1)} all-to-all(bf16[8,2,1024]{2,1,0:T(2,128)(2,1)S(1)} %reshape.163), channel_id=1, replica_groups=mesh['ep'=8,'tp'=4] {'ep'}, dimensions={0} | all-to-all | bytes 65536 | tf_op jit(solution)/shard_map/all_to_all | solution.py:91
  110.1 0.0 copy-done.1
  110.1 0.3 convolution_bitcast_fusion.1
  110.4 0.0 copy-done.2
  110.4 0.0 copy-done.3
  110.4 1.3 fusion.1
  111.7 0.0 reduce-scatter.2.cloned.1.call-update
  111.7 0.0 copy-done.8
  111.8 17.1 %reduce-scatter.2.cloned.1.call-done = bf16[8,1,512]{2,0,1:T(8,128)(2,1)} async-done(((bf16[8,1,2048]{2,0,1:T(8,128)(2,1)}), bf16[8,1,512]{2,0,1:T(8,128)(2,1)}) %reduce-scatter.2.cloned.1.call-update) | async-done | bytes 8208 | tf_op jit(solution)/shard_map/reduce_scatter | solution.py:97
  128.9 1.3 reduce.3
  130.2 0.6 reshape.165
  130.9 5.5 %all-to-all-start.2 = ((bf16[8,2,256]{2,1,0:T(2,128)(2,1)}), bf16[8,2,256]{2,1,0:T(2,128)(2,1)S(1)}, u32[]{:S(2)}, u32[]{:S(2)}) async-start(bf16[8,2,256]{2,1,0:T(2,128)(2,1)} %reshape.165), calls=%async_computation.3 | async-start | bytes 16384 | tf_op jit(solution)/shard_map/all_to_all | solution.py:100
  136.4 0.0 copy-done.7
  136.4 0.1 select_reduce_fusion
  136.5 6.4 %all-to-all-done.2 = bf16[8,2,256]{2,1,0:T(2,128)(2,1)S(1)} async-done(((bf16[8,2,256]{2,1,0:T(2,128)(2,1)}), bf16[8,2,256]{2,1,0:T(2,128)(2,1)S(1)}, u32[]{:S(2)}, u32[]{:S(2)}) %all-to-all-start.2) | async-done | bytes 8224 | tf_op jit(solution)/shard_map/all_to_all | solution.py:100
  142.9 0.7 fusion.4
  (11 shorter events, 0.2 us)
Async XLA Ops:
  6.5 55.8 %copy-start = (bf16[4,1,1024,128]{3,2,1,0:T(8,128)(2,1)S(1)}, bf16[4,1,1024,128]{3,2,1,0:T(8,128)(2,1)}, u32[]{:S(2)}) copy-start(bf16[4,1,1024,128]{3,2,1,0:T(8,128)(2,1)} %param.19) | copy-start | bytes 3145732
  6.5 80.1 %all-gather.2.cloned.1.call-start = ((), (), s32[]{:S(2)}) async-start(), calls=%async_computation.4 | async-start | bytes 2359296 | tf_op jit(solution)/shard_map/all_gather | solution.py:71
  9.5 14.0 %all-to-all-start = ((bf16[4,8,256]{2,0,1:T(4,128)(2,1)}), bf16[4,8,256]{2,0,1:T(4,128)(2,1)S(1)}, u32[]{:S(2)}, u32[]{:S(2)}) async-start(bf16[4,8,256]{2,0,1:T(4,128)(2,1)} %bitcast), calls=%async_computation | async-start | bytes 32768 | tf_op jit(solution)/shard_map/all_to_all | solution.py:37
  16.8 112.1 %reduce-scatter.2.cloned.1.call-start = ((), (), s32[]{:S(2)}) async-start(), calls=%async_computation.5 | async-start | bytes 40960 | tf_op jit(solution)/shard_map/reduce_scatter | solution.py:97
  18.2 5.3 %copy-start.6 = (s32[4,2]{0,1:T(2,128)}, s32[4,2]{0,1:T(2,128)S(1)}, u32[]{:S(2)}) copy-start(s32[4,2]{0,1:T(2,128)S(1)} %broadcast_add_fusion) | copy-start | bytes 100
  18.9 43.8 %copy-start.5 = (pred[4,1024]{1,0:T(4,128)(4,1)}, pred[4,1024]{1,0:T(4,128)(4,1)S(1)}, u32[]{:S(2)}) copy-start(pred[4,1024]{1,0:T(4,128)(4,1)S(1)} %iota_compare_fusion) | copy-start | bytes 12292
  62.8 36.0 %copy-start.4 = (bf16[4,2048]{1,0:T(4,128)(2,1)S(1)}, bf16[4,2048]{1,0:T(4,128)(2,1)}, u32[]{:S(2)}) copy-start(bf16[4,2048]{1,0:T(4,128)(2,1)} %param.15) | copy-start | bytes 49156
  83.5 26.6 %copy-start.1 = (bf16[1,2048,192]{1,2,0:T(8,128)(2,1)S(1)}, bf16[1,2048,192]{1,2,0:T(8,128)(2,1)}, u32[]{:S(2)}) copy-start(bf16[1,2048,192]{1,2,0:T(8,128)(2,1)} %param.27) | copy-start | bytes 2359300
  84.3 26.2 %copy-start.2 = (bf16[1,192,2048]{2,1,0:T(8,128)(2,1)S(1)}, bf16[1,192,2048]{2,1,0:T(8,128)(2,1)}, u32[]{:S(2)}) copy-start(bf16[1,192,2048]{2,1,0:T(8,128)(2,1)} %param.29) | copy-start | bytes 2359300
  84.3 26.2 %copy-start.3 = (bf16[1,2048,192]{1,2,0:T(8,128)(2,1)S(1)}, bf16[1,2048,192]{1,2,0:T(8,128)(2,1)}, u32[]{:S(2)}) copy-start(bf16[1,2048,192]{1,2,0:T(8,128)(2,1)} %param.28) | copy-start | bytes 2359300
  86.6 25.1 %copy-start.8 = (bf16[4,2]{0,1:T(2,128)(2,1)S(1)}, bf16[4,2]{0,1:T(2,128)(2,1)}, u32[]{:S(2)}) copy-start(bf16[4,2]{0,1:T(2,128)(2,1)} %param.26) | copy-start | bytes 52
  86.6 49.8 %copy-start.7 = (s32[4,2]{0,1:T(2,128)S(1)}, s32[4,2]{0,1:T(2,128)}, u32[]{:S(2)}) copy-start(s32[4,2]{0,1:T(2,128)} %copy-done.6) | copy-start | bytes 100
  130.9 12.0 %all-to-all-start.2 = ((bf16[8,2,256]{2,1,0:T(2,128)(2,1)}), bf16[8,2,256]{2,1,0:T(2,128)(2,1)S(1)}, u32[]{:S(2)}, u32[]{:S(2)}) async-start(bf16[8,2,256]{2,1,0:T(2,128)(2,1)} %reshape.165), calls=%async_computation.3 | async-start | bytes 16384 | tf_op jit(solution)/shard_map/all_to_all | solution.py:100
Sparse Core Ops, SparseCore 0:
  9.4 54.2 all-gather.1
  111.9 16.9 reduce-scatter.1
where the time goes:
time: 151 us; the launch traced here: 150 us
  blocking collectives  56.9 us (38%)
  other arithmetic  27.7 us (18%)
  waiting for transfers between devices  25.6 us (17%)
  between operations  14.1 us (9%)
  starting transfers between devices  12.8 us (8%)
  matrix products  9.09 us (6%)
  local copies, waits for them, and re-layouts  4.21 us (3%)
    unnamed x1, blocking collectives  37.7 us
    another operation x2, other arithmetic  20.5 us
    reduce_scatter x1, waiting for transfers between devices, body(): lax.psum_scatter(down_rounded.astype(jnp.bfloat16), 'tp', scatter_dimensi...  17.1 us
    psum x1, blocking collectives, body(): attended = lax.psum(rounded.astype(jnp.bfloat16), 'tp').astype(jnp.float32)  10.1 us
    all_to_all x1, blocking collectives, body(): lax.all_to_all(outgoing, 'ep', split_axis=0, concat_axis=0, tiled=True)  9.06 us
    all_to_all x1, starting transfers between devices, body(): lax.all_to_all(normed, 'ep', split_axis=1, concat_axis=0, tiled=True)  7.28 us
    all_to_all x1, waiting for transfers between devices, body(): lax.all_to_all(summed, 'ep', split_axis=0, concat_axis=0, tiled=True)  6.43 us
    all_to_all x1, starting transfers between devices, body(): lax.all_to_all(summed, 'ep', split_axis=0, concat_axis=0, tiled=True)  5.51 us
  transfers between devices with their start and end apart: 4, of which 3 were waited for; matrix products, arithmetic and copies ran while one was open for 22% of the time, Pallas kernels for 0%

commit v1 on v0

--- a/solution.py
+++ b/solution.py
@@ -4,6 +4,11 @@
 from jax.sharding import PartitionSpec as P
 
 rms_epsilon = 1e-06
+
+
+def cover_groups(local_x):
+    wide_out = lax.all_gather(local_x, axis_name="tp").sum(axis=0)
+    return wide_out
 
 
 def rms_scale(values, gain):
@@ -72,7 +77,7 @@
         preferred_element_type=jnp.float32,
     )
     rounded = lax.optimization_barrier(partial_value.astype(jnp.bfloat16)).astype(jnp.float32)
-    attended = lax.psum(rounded.astype(jnp.bfloat16), "tp").astype(jnp.float32)
+    attended = cover_groups(rounded.astype(jnp.bfloat16)).astype(jnp.float32)
     residual = (hidden.astype(jnp.float32) + attended).astype(jnp.bfloat16)
     normed_two = rms_scale(residual, moe_gain)
     per_device = gate_w.shape[0]

time: 151 us -> 143 us (0.947)
  blocking collectives: 56.9 us -> 51.5 us
  matrix products: 9.09 us -> 6.49 us
    psum x1 -> x0, blocking collectives: 10.1 us -> none  [body(): attended = lax.psum(rounded.astype(jnp.bfloat16), 'tp').astype(jnp.float32)]
    all_gather x0 -> x1, blocking collectives: none -> 5.23 us  [cover_groups(): wide_out = lax.all_gather(local_x, axis_name='tp').sum(axis=0)]
    dot_general x1, matrix products: 2.35 us -> 0.36 us  [body(): jnp.einsum('tkgp,tkpd->tkgd', weight, value_cache, preferred_element_type...]
  transfers between devices with their start and end apart: 4 -> 4, of which waited for: 3 -> 3; matrix products, arithmetic and copies ran while one was open for 22% -> 21% of each run, Pallas kernels for 0% -> 0%
where the time goes in v1:
time: 143 us; the launch traced here: 142 us
  blocking collectives  51.5 us (36%)
  other arithmetic  27.2 us (19%)
  waiting for transfers between devices  26 us (18%)
  between operations  14.2 us (10%)
  starting transfers between devices  12.8 us (9%)
  matrix products  6.49 us (5%)
  local copies, waits for them, and re-layouts  3.55 us (2%)
    unnamed x1, blocking collectives  37.2 us
    another operation x2, other arithmetic  20.5 us
    reduce_scatter x1, waiting for transfers between devices, body(): lax.psum_scatter(down_rounded.astype(jnp.bfloat16), 'tp', scatter_dimensi...  17 us
    all_to_all x1, blocking collectives, body(): lax.all_to_all(outgoing, 'ep', split_axis=0, concat_axis=0, tiled=True)  9.06 us
    all_to_all x1, starting transfers between devices, body(): lax.all_to_all(normed, 'ep', split_axis=1, concat_axis=0, tiled=True)  7.28 us
    all_to_all x1, waiting for transfers between devices, body(): lax.all_to_all(summed, 'ep', split_axis=0, concat_axis=0, tiled=True)  6.44 us
    all_to_all x1, starting transfers between devices, body(): lax.all_to_all(summed, 'ep', split_axis=0, concat_axis=0, tiled=True)  5.51 us
    all_gather x1, blocking collectives, cover_groups(): wide_out = lax.all_gather(local_x, axis_name='tp').sum(axis=0)  5.23 us
  transfers between devices with their start and end apart: 4, of which 3 were waited for; matrix products, arithmetic and copies ran while one was open for 21% of the time, Pallas kernels for 0%

profile of v1, /device:TPU:0, one launch (start us, length us, event | category | flops | bytes accessed | tf_op | source)
XLA Modules:
  0.0 141.9 jit_solution(7151724625158090439)
XLA Ops:
  6.5 0.0 copy-start
  6.5 0.0 copy-start.5
  6.5 0.0 all-gather.4.cloned.1.call-start
  6.5 0.7 all-gather.4.cloned.1.call-update
  7.3 0.8 fusion.25
  8.1 1.4 fusion.27
  9.5 7.3 %all-to-all-start = ((bf16[4,8,256]{2,0,1:T(4,128)(2,1)}), bf16[4,8,256]{2,0,1:T(4,128)(2,1)S(1)}, u32[]{:S(2)}, u32[]{:S(2)}) async-start(bf16[4,8,256]{2,0,1:T(4,128)(2,1)} %bitcast), calls=%async_computation | async-start | bytes 32768 | tf_op jit(solution)/shard_map/all_to_all | solution.py:42
  16.8 0.0 reduce-scatter.2.cloned.1.call-start
  16.8 0.7 broadcast_multiply_fusion
  17.5 0.7 broadcast_add_fusion
  18.2 0.7 iota_compare_fusion
  18.9 0.1 fusion.51
  19.0 0.7 dynamic_slice.6
  19.7 1.2 dynamic-slice
  21.6 1.9 %all-to-all-done = bf16[4,8,256]{2,0,1:T(4,128)(2,1)S(1)} async-done(((bf16[4,8,256]{2,0,1:T(4,128)(2,1)}), bf16[4,8,256]{2,0,1:T(4,128)(2,1)S(1)}, u32[]{:S(2)}, u32[]{:S(2)}) %all-to-all-start) | async-done | bytes 16416 | tf_op jit(solution)/shard_map/all_to_all | solution.py:42
  23.5 1.1 fusion.57
  24.6 37.2 %all-reduce = bf16[32,512]{1,0:T(8,128)(2,1)S(1)} all-reduce(f32[32,512]{1,0:T(8,128)S(1)} %fusion.57), channel_id=3, replica_groups=mesh['ep'=8,'tp'=4] {'ep'}, use_global_device_ids=true, to_apply=%region_1.0.clone | all-reduce | flops 16384 | bytes 98304
  61.8 0.0 copy-done
  61.9 0.4 fusion.21
  62.3 19.8 %reduce-window.6 = f32[4,1,4,8,128]{4,3,2,1,0:T(8,128)S(1)} reduce-window(f32[4,1,4,8,128]{4,3,2,1,0:T(8,128)S(1)} %bitcast.83, f32[]{:T(128)} %constant.13.clone.1), window={size=1x1x1x1x128 pad=0_0x0_0x0_0x0_0x0_127}, to_apply=%region_2.3 | reduce-window | flops 2080768 | bytes 131076 | tf_op jit(solution)/shard_map/reduce-window
  82.1 0.0 copy-start.4
  82.1 0.0 copy-start.6
  82.2 0.1 slice_reduce_fusion
  82.3 0.7 reduce-window.9
  83.0 0.1 slice_bitcast_fusion
  83.1 0.1 broadcast.72
  83.2 0.0 copy-start.1
  83.2 0.0 copy-done.5
  83.2 0.4 fusion.6
  83.6 0.0 copy-start.2
  83.6 0.0 copy-start.3
  83.6 0.0 copy-start.7
  83.6 0.0 all-gather.4.cloned.1.call-done
  83.6 2.1 %convolution_convert_fusion.2 = bf16[4,2048]{1,0:T(4,128)(2,1)S(1)} fusion(bf16[512,2048]{1,0:T(8,128)(2,1)} %all-gather.4.cloned.1.call-done, bf16[1,4,4,128]{3,2,1,0:T(4,128)(2,1)S(1)} %fusion.6), kind=kOutput, calls=%fused_computation.4 | convolution fusion | flops 8396800 | bytes 2117632 | tf_op jit(solution)/shard_map/dot_general | solution.py:74
  85.7 5.2 %all-gather.1 = bf16[4,4,2048]{2,1,0:T(4,128)(2,1)S(1)} all-gather(bf16[1,4,2048]{2,1,0:T(4,128)(2,1)S(1)} %bitcast.84), channel_id=2, replica_groups=mesh['ep'=8,'tp'=4] {'tp'}, dimensions={0}, use_global_device_ids=true | all-gather | bytes 81920 | tf_op jit(solution)/shard_map/all_gather | solution.py:10
  91.0 0.0 copy-done.4
  91.0 0.1 fusion.22
  91.1 0.0 copy-done.6
  91.1 0.2 fusion
  91.3 0.5 broadcast.80
  91.9 0.7 reduce.4
  92.5 9.1 %all_to_all.29 = bf16[8,2,1024]{2,1,0:T(2,128)(2,1)S(1)} all-to-all(bf16[8,2,1024]{2,1,0:T(2,128)(2,1)S(1)} %reshape.167), channel_id=1, replica_groups=mesh['ep'=8,'tp'=4] {'ep'}, dimensions={0} | all-to-all | bytes 65536 | tf_op jit(solution)/shard_map/all_to_all | solution.py:96
  101.6 0.0 copy-done.1
  101.7 0.3 convolution_bitcast_fusion.1
  102.0 0.0 copy-done.2
  102.0 0.0 copy-done.3
  102.0 1.3 fusion.1
  103.3 0.0 reduce-scatter.2.cloned.1.call-update
  103.3 0.0 copy-done.7
  103.3 17.0 %reduce-scatter.2.cloned.1.call-done = bf16[8,1,512]{2,0,1:T(8,128)(2,1)} async-done(((bf16[8,1,2048]{2,0,1:T(8,128)(2,1)}), bf16[8,1,512]{2,0,1:T(8,128)(2,1)}) %reduce-scatter.2.cloned.1.call-update) | async-done | bytes 8208 | tf_op jit(solution)/shard_map/reduce_scatter | solution.py:102
  120.3 1.3 reduce.5
  121.7 0.6 reshape.169
  122.3 5.5 %all-to-all-start.2 = ((bf16[8,2,256]{2,1,0:T(2,128)(2,1)}), bf16[8,2,256]{2,1,0:T(2,128)(2,1)S(1)}, u32[]{:S(2)}, u32[]{:S(2)}) async-start(bf16[8,2,256]{2,1,0:T(2,128)(2,1)} %reshape.169), calls=%async_computation.3 | async-start | bytes 16384 | tf_op jit(solution)/shard_map/all_to_all | solution.py:105
  127.8 0.1 select_reduce_fusion
  127.9 6.4 %all-to-all-done.2 = bf16[8,2,256]{2,1,0:T(2,128)(2,1)S(1)} async-done(((bf16[8,2,256]{2,1,0:T(2,128)(2,1)}), bf16[8,2,256]{2,1,0:T(2,128)(2,1)S(1)}, u32[]{:S(2)}, u32[]{:S(2)}) %all-to-all-start.2) | async-done | bytes 8224 | tf_op jit(solution)/shard_map/all_to_all | solution.py:105
  134.3 0.7 fusion.4
  (13 shorter events, 0.2 us)
Async XLA Ops:
  6.5 55.3 %copy-start = (bf16[4,1,1024,128]{3,2,1,0:T(8,128)(2,1)S(1)}, bf16[4,1,1024,128]{3,2,1,0:T(8,128)(2,1)}, u32[]{:S(2)}) copy-start(bf16[4,1,1024,128]{3,2,1,0:T(8,128)(2,1)} %param.19) | copy-start | bytes 3145732
  6.5 76.7 %copy-start.5 = (bf16[4,1,1024,128]{3,2,1,0:T(8,128)(2,1)S(1)}, bf16[4,1,1024,128]{3,2,1,0:T(8,128)(2,1)}, u32[]{:S(2)}) copy-start(bf16[4,1,1024,128]{3,2,1,0:T(8,128)(2,1)} %param.20) | copy-start | bytes 3145732
  6.5 77.1 %all-gather.4.cloned.1.call-start = ((), (), s32[]{:S(2)}) async-start(), calls=%async_computation.4 | async-start | bytes 2359296 | tf_op jit(solution)/shard_map/all_gather | solution.py:76
  9.5 14.0 %all-to-all-start = ((bf16[4,8,256]{2,0,1:T(4,128)(2,1)}), bf16[4,8,256]{2,0,1:T(4,128)(2,1)S(1)}, u32[]{:S(2)}, u32[]{:S(2)}) async-start(bf16[4,8,256]{2,0,1:T(4,128)(2,1)} %bitcast), calls=%async_computation | async-start | bytes 32768 | tf_op jit(solution)/shard_map/all_to_all | solution.py:42
  16.8 103.5 %reduce-scatter.2.cloned.1.call-start = ((), (), s32[]{:S(2)}) async-start(), calls=%async_computation.5 | async-start | bytes 40960 | tf_op jit(solution)/shard_map/reduce_scatter | solution.py:102
  82.1 8.8 %copy-start.4 = (bf16[4,2048]{1,0:T(4,128)(2,1)S(1)}, bf16[4,2048]{1,0:T(4,128)(2,1)}, u32[]{:S(2)}) copy-start(bf16[4,2048]{1,0:T(4,128)(2,1)} %param.15) | copy-start | bytes 49156
  82.1 9.0 %copy-start.6 = (f32[2048]{0:T(1024)S(1)}, f32[2048]{0:T(1024)}, u32[]{:S(2)}) copy-start(f32[2048]{0:T(1024)} %param.23) | copy-start | bytes 24580
  83.2 18.4 %copy-start.1 = (bf16[1,2048,192]{1,2,0:T(8,128)(2,1)S(1)}, bf16[1,2048,192]{1,2,0:T(8,128)(2,1)}, u32[]{:S(2)}) copy-start(bf16[1,2048,192]{1,2,0:T(8,128)(2,1)} %param.27) | copy-start | bytes 2359300
  83.6 18.4 %copy-start.2 = (bf16[1,192,2048]{2,1,0:T(8,128)(2,1)S(1)}, bf16[1,192,2048]{2,1,0:T(8,128)(2,1)}, u32[]{:S(2)}) copy-start(bf16[1,192,2048]{2,1,0:T(8,128)(2,1)} %param.29) | copy-start | bytes 2359300
  83.6 18.4 %copy-start.3 = (bf16[1,2048,192]{1,2,0:T(8,128)(2,1)S(1)}, bf16[1,2048,192]{1,2,0:T(8,128)(2,1)}, u32[]{:S(2)}) copy-start(bf16[1,2048,192]{1,2,0:T(8,128)(2,1)} %param.28) | copy-start | bytes 2359300
  83.6 19.7 %copy-start.7 = (bf16[4,2]{0,1:T(2,128)(2,1)S(1)}, bf16[4,2]{0,1:T(2,128)(2,1)}, u32[]{:S(2)}) copy-start(bf16[4,2]{0,1:T(2,128)(2,1)} %param.26) | copy-start | bytes 52
  122.3 12.0 %all-to-all-start.2 = ((bf16[8,2,256]{2,1,0:T(2,128)(2,1)}), bf16[8,2,256]{2,1,0:T(2,128)(2,1)S(1)}, u32[]{:S(2)}, u32[]{:S(2)}) async-start(bf16[8,2,256]{2,1,0:T(2,128)(2,1)} %reshape.169), calls=%async_computation.3 | async-start | bytes 16384 | tf_op jit(solution)/shard_map/all_to_all | solution.py:105
Sparse Core Ops, SparseCore 0:
  9.4 53.7 all-gather.3
  103.4 16.8 reduce-scatter.1
